TPU v7x, 32 devices: a whole 2x2x4 slice. The times are simulated.
32 devices in a mesh: fs: 4 (over z), rep: 4 (over y, x), tp: 2 (over core).
Axes of the slice: x: 2, y: 2, z: 4, core: 2. Of those that a mesh axis runs over, the one named last changes fastest.
Arguments:
- input_act: bfloat16 [12288, 2048], P(('fs', 'rep')), may hold values from -6 to 6
- query_cot: bfloat16 [12288, 1024], P(('fs', 'rep'), 'tp'), may hold values from -6 to 6
- out_cot: bfloat16 [12288, 2048], P(('fs', 'rep')), may hold values from -6 to 6
- attn_out: bfloat16 [12288, 1024], P(('fs', 'rep'), 'tp'), may hold values from -6 to 6
- query_w: float32 [2048, 1024], P('fs', 'tp'), may hold values from -0.125 to 0.125
- out_w: float32 [1024, 2048], P('tp', 'fs'), may hold values from -0.1875 to 0.1875
- query_factor: bfloat16 [2048, 512], P('fs'), may hold values from -0.125 to 0.125
- out_factor: bfloat16 [2048, 512], P('fs'), may hold values from -0.125 to 0.125
- first_q: float32 [512, 1024], P('fs', 'tp'), may hold values from -6 to 6
- second_q: float32 [512, 1024], P('fs', 'tp'), may hold values from 0.075 to 120
- first_o: float32 [512, 1024], P('fs', 'tp'), may hold values from -6 to 6
- second_o: float32 [512, 1024], P('fs', 'tp'), may hold values from 0.075 to 120
Outputs:
- new_query_w: float32 [2048, 1024], P('fs', 'tp')
- new_out_w: float32 [1024, 2048], P('tp', 'fs')
- query_step: float32 [2048, 1024], P('fs', 'tp')
- out_step: float32 [1024, 2048], P('tp', 'fs')
- new_first_q: float32 [512, 1024], P('fs', 'tp')
- new_second_q: float32 [512, 1024], P('fs', 'tp')
- new_first_o: float32 [512, 1024], P('fs', 'tp')
- new_second_o: float32 [512, 1024], P('fs', 'tp')
- query_copy: bfloat16 [2048, 1024], P(None, 'tp')
- out_copy: bfloat16 [1024, 2048], P('tp')
All inputs are finite; a program needn't handle non-finite values.
Results may differ from a plain program's by a relative error of at most 0.0085.
Values may be sent and summed in bfloat16 or wider, within the bound.
A program may use at most 64 MiB of HBM per device.

v0:
```python
import math
import jax
import jax.numpy as jnp
from jax import lax
from jax.sharding import PartitionSpec as P

RANK = 512
HQ = 1024


def contract_rows(left_side, right_side):
    return lax.dot_general(
        left_side, right_side, (((0,), (0,)), ((), ())), preferred_element_type=jnp.float32
    )


def contract_exact(left_side, right_side):
    return lax.dot_general(
        left_side.astype(jnp.float32),
        right_side,
        (((0,), (0,)), ((), ())),
        precision=lax.Precision.HIGHEST,
        preferred_element_type=jnp.float32,
    )


def exact_dot(left_side, right_side):
    return jnp.dot(
        left_side, right_side, precision=lax.Precision.HIGHEST, preferred_element_type=jnp.float32
    )


def body(
    input_act,
    query_cot,
    out_cot,
    attn_out,
    query_w,
    out_w,
    query_factor,
    out_factor,
    first_q,
    second_q,
    first_o,
    second_o,
):
    heads_local = query_cot.shape[1]
    token_total = input_act.shape[0] * lax.axis_size("fs") * lax.axis_size("rep")
    scale_tokens = 1.0 / math.sqrt(token_total)
    gradient = lax.psum_scatter(
        jnp.concatenate(
            [contract_rows(input_act, query_cot), contract_rows(out_cot, attn_out)], axis=1
        ).astype(jnp.bfloat16),
        "fs",
        scatter_dimension=0,
        tiled=True,
    ).astype(jnp.float32)
    partial_value = jnp.concatenate(
        [
            contract_exact(query_factor, gradient[:, :heads_local]),
            contract_exact(out_factor, gradient[:, heads_local:]),
        ],
        axis=1,
    )
    projected = lax.psum_scatter(
        partial_value.astype(jnp.bfloat16), "fs", scatter_dimension=0, tiled=True
    ).astype(jnp.float32)
    projected = lax.psum(projected.astype(jnp.bfloat16), "rep").astype(jnp.float32) * scale_tokens
    proj_q = projected[:, :heads_local]
    proj_o = projected[:, heads_local:]
    new_first_q = 0.8 * first_q + 0.2 * proj_q
    new_second_q = 0.9 * second_q + 0.1 * proj_q * proj_q
    new_first_o = 0.8 * first_o + 0.2 * proj_o
    new_second_o = 0.9 * second_o + 0.1 * proj_o * proj_o
    dir_q = new_first_q / jnp.sqrt(new_second_q)
    dir_o = new_first_o / jnp.sqrt(new_second_o)
    local_squares = jnp.sum(dir_q * dir_q) + jnp.sum(dir_o * dir_o)
    total_squares = lax.psum(local_squares, ("fs", "tp"))
    norm_scale = jnp.sqrt(total_squares / (2 * RANK * HQ) + 1e-06)
    whole_dir_q, whole_dir_o = (
        lax.all_gather(dir_q, "fs", axis=0, tiled=True),
        lax.all_gather(dir_o, "fs", axis=0, tiled=True),
    )
    query_step = exact_dot(query_factor.astype(jnp.float32), whole_dir_q) / norm_scale
    out_step = (exact_dot(out_factor.astype(jnp.float32), whole_dir_o) / norm_scale).T
    new_query_w = query_w - 0.01 * query_step
    new_out_w = out_w - 0.01 * out_step
    query_copy = lax.all_gather(new_query_w.astype(jnp.bfloat16), "fs", axis=0, tiled=True)
    out_copy = lax.all_gather(new_out_w.astype(jnp.bfloat16), "fs", axis=1, tiled=True)
    return (
        new_query_w,
        new_out_w,
        query_step,
        out_step,
        new_first_q,
        new_second_q,
        new_first_o,
        new_second_o,
        query_copy,
        out_copy,
    )


def solution(mesh):
    return jax.shard_map(
        body,
        mesh=mesh,
        in_specs=(
            P(("fs", "rep"), None),
            P(("fs", "rep"), "tp"),
            P(("fs", "rep"), None),
            P(("fs", "rep"), "tp"),
            P("fs", "tp"),
            P("tp", "fs"),
            P("fs", None),
            P("fs", None),
            P("fs", "tp"),
            P("fs", "tp"),
            P("fs", "tp"),
            P("fs", "tp"),
        ),
        out_specs=(
            P("fs", "tp"),
            P("tp", "fs"),
            P("fs", "tp"),
            P("tp", "fs"),
            P("fs", "tp"),
            P("fs", "tp"),
            P("fs", "tp"),
            P("fs", "tp"),
            P(None, "tp"),
            P("tp", None),
        ),
        check_vma=False,
    )
```

profile of v0, /device:TPU:0, one launch (start us, length us, event | category | flops | bytes accessed | tf_op | source)
XLA Modules:
  0.0 343.3 jit_solution(11248011831809214401)
XLA Ops:
  7.2 1.8 copy-done
  9.1 3.1 convolution_convert_fusion.1
  12.2 1.9 convolution_convert_fusion
  14.1 2.5 pad_maximum_fusion
  16.8 79.6 %reduce-scatter.5.cloned.1.call-done = bf16[512,1024]{0,1:T(8,128)(2,1)} async-done(((bf16[2048,1024]{0,1:T(8,128)(2,1)}), bf16[512,1024]{0,1:T(8,128)(2,1)}) %reduce-scatter.5.cloned.1.call-update) | async-done | bytes 1048592 | tf_op jit(solution)/shard_map/reduce_scatter | solution.py:50
  98.0 1.6 fusion.1
  100.7 2.3 copy.59
  103.0 27.9 %reduce-scatter.7.cloned.1.call-done = bf16[128,1024]{1,0:T(8,128)(2,1)} async-done(((bf16[512,1024]{1,0:T(8,128)(2,1)}), bf16[128,1024]{1,0:T(8,128)(2,1)}) %reduce-scatter.7.cloned.1.call-update) | async-done | bytes 262160
  130.9 1.8 copy.60
  133.7 1.8 copy.41
  135.4 1.8 copy.42
  137.2 1.8 copy.43
  139.0 37.0 %all-reduce.2.cloned.1.call-done = bf16[128,1024]{0,1:T(8,128)(2,1)} async-done(((bf16[128,1024]{0,1:T(8,128)(2,1)}), bf16[128,1024]{0,1:T(8,128)(2,1)}) %all-reduce.2.cloned.1.call-update) | async-done | bytes 262160 | tf_op jit(solution)/shard_map/psum | solution.py:68
  177.0 2.9 multiply_reduce_fusion
  181.9 2.5 copy.45
  184.4 16.9 %psum.15 = f32[]{:T(128)} all-reduce(f32[]{:T(128)S(6)} %add.30), channel_id=1, replica_groups=mesh['fs'=4,'rep'=4,'tp'=2] {'fs','tp'}, use_global_device_ids=true, to_apply=%region_5.0 | all-reduce | flops 1 | bytes 8 | tf_op jit(solution)/shard_map/psum | solution.py:78
  202.0 8.3 %all-gather.5.cloned.1.call-done = f32[512,512]{0,1:T(8,128)} async-done(((f32[128,512]{0,1:T(8,128)}), f32[512,512]{0,1:T(8,128)}) %all-gather.5.cloned.1.call-update) | async-done | bytes 1048592 | tf_op jit(solution)/shard_map/all_gather | solution.py:81
  210.3 4.2 %fusion.8 = (bf16[512,512]{0,1:T(8,128)(2,1)}, f32[512,512]{0,1:T(8,128)}, f32[512,512]{0,1:T(8,128)}) fusion(f32[512,512]{0,1:T(8,128)} %copy.45, f32[]{:T(128)S(6)} %sqrt.11, f32[512,512]{0,1:T(8,128)} %all-gather.5.cloned.1.call-done, bf16[512,512]{1,0:T(8,128)(2,1)} %param.18), kind=kOutput, calls=%fused_computation.27 | convolution fusion | flops 1611661312 | bytes 5242884 | tf_op jit(solution)/shard_map/dot_general | solution.py:28
  214.6 2.5 copy.47
  217.1 23.4 %all-gather.7.cloned.1.call-done = f32[512,512]{0,1:T(8,128)} async-done(((f32[128,512]{0,1:T(8,128)}), f32[512,512]{0,1:T(8,128)}) %all-gather.7.cloned.1.call-update) | async-done | bytes 1048592 | tf_op jit(solution)/shard_map/all_gather | solution.py:82
  240.5 4.3 %fusion.7 = (bf16[512,512]{0,1:T(8,128)(2,1)}, f32[512,512]{0,1:T(8,128)}, f32[512,512]{0,1:T(8,128)}) fusion(f32[512,512]{0,1:T(8,128)} %copy.47, f32[]{:T(128)S(6)} %sqrt.11, f32[512,512]{0,1:T(8,128)} %all-gather.7.cloned.1.call-done, bf16[512,512]{1,0:T(8,128)(2,1)} %param.19), kind=kOutput, calls=%fused_computation.26 | convolution fusion | flops 1611661312 | bytes 5242884 | tf_op jit(solution)/shard_map/dot_general | solution.py:28
  244.9 1.8 copy.55
  246.6 1.8 copy.54
  248.4 1.8 copy.53
  251.1 2.5 copy.49
  253.6 2.5 copy.51
  256.1 2.5 copy.48
  258.7 2.5 copy.50
  261.2 25.3 %all-gather.9.cloned.1.call-done = bf16[2048,512]{0,1:T(8,128)(2,1)} async-done(((bf16[512,512]{0,1:T(8,128)(2,1)}), bf16[2048,512]{0,1:T(8,128)(2,1)}) %all-gather.9.cloned.1.call-update) | async-done | bytes 2097168 | tf_op jit(solution)/shard_map/all_gather | solution.py:88
  286.5 3.9 %copy.56 = bf16[2048,512]{1,0:T(8,128)(2,1)} copy(bf16[2048,512]{0,1:T(8,128)(2,1)} %all-gather.9.cloned.1.call-done) | data formatting | bytes 4194304
  290.4 42.1 %all-gather.11.cloned.1.call-done = bf16[512,2048]{0,1:T(8,128)(2,1)} async-done(((bf16[512,512]{0,1:T(8,128)(2,1)}), bf16[512,2048]{0,1:T(8,128)(2,1)}) %all-gather.11.cloned.1.call-update) | async-done | bytes 2097168 | tf_op jit(solution)/shard_map/all_gather | solution.py:89
  332.6 3.9 %copy.57 = bf16[512,2048]{1,0:T(8,128)(2,1)} copy(bf16[512,2048]{0,1:T(8,128)(2,1)} %all-gather.11.cloned.1.call-done) | data formatting | bytes 4194304
  (26 shorter events, 6.3 us)
Async XLA Ops:
  7.2 1.9 copy-start
  7.2 89.2 %reduce-scatter.5.cloned.1.call-start = ((), (), s32[]{:S(2)}) async-start(), calls=%async_computation.2 | async-start | bytes 5242880 | tf_op jit(solution)/shard_map/reduce_scatter | solution.py:50
  9.1 3.1 copy-start.2
  9.1 3.1 copy-start.3
  16.7 114.2 %reduce-scatter.7.cloned.1.call-start = ((), (), s32[]{:S(2)}) async-start(), calls=%async_computation.8 | async-start | bytes 1310720
  99.7 33.2 %copy-start.1 = (f32[128,512]{1,0:T(8,128)S(1)}, f32[128,512]{1,0:T(8,128)}, u32[]{:S(2)}) copy-start(f32[128,512]{1,0:T(8,128)} %param.20) | copy-start | bytes 786436
  103.0 73.0 %all-reduce.2.cloned.1.call-start = ((), (), s32[]{:S(2)}) async-start(), calls=%async_computation.3 | async-start | bytes 524288 | tf_op jit(solution)/shard_map/psum | solution.py:68
  132.8 77.5 %all-gather.5.cloned.1.call-start = ((), (), s32[]{:S(2)}) async-start(), calls=%async_computation.4 | async-start | bytes 1310720 | tf_op jit(solution)/shard_map/all_gather | solution.py:81
  179.9 60.6 %all-gather.7.cloned.1.call-start = ((), (), s32[]{:S(2)}) async-start(), calls=%async_computation.5 | async-start | bytes 1310720 | tf_op jit(solution)/shard_map/all_gather | solution.py:82
  180.5 106.0 %all-gather.9.cloned.1.call-start = ((), (), s32[]{:S(2)}) async-start(), calls=%async_computation.6 | async-start | bytes 2621440 | tf_op jit(solution)/shard_map/all_gather | solution.py:88
  214.6 118.0 %all-gather.11.cloned.1.call-start = ((), (), s32[]{:S(2)}) async-start(), calls=%async_computation.7 | async-start | bytes 2621440 | tf_op jit(solution)/shard_map/all_gather | solution.py:89
Sparse Core Ops, SparseCore 0:
  16.8 79.5 reduce-scatter.4
  103.1 27.7 reduce-scatter.6
  134.4 41.5 all-reduce.1
  180.1 30.1 all-gather.4
  212.3 28.2 all-gather.6
  242.5 43.9 all-gather.8
  288.1 44.4 all-gather.10
where the time goes:
time: 344 us; the launch traced here: 343 us
  waiting for transfers between devices  244 us (71%)
  local copies, waits for them, and re-layouts  41.3 us (12%)
  blocking collectives  16.9 us (5%)
  matrix products  16.8 us (5%)
  between operations  16.2 us (5%)
  other arithmetic  7.46 us (2%)
    reduce_scatter x1, waiting for transfers between devices, body(): lax.psum_scatter(jnp.concatenate([contract_rows(input_act, query_cot), co...  79.6 us
    all_gather x1, waiting for transfers between devices, body(): lax.all_gather(new_out_w.astype(jnp.bfloat16), 'fs', axis=1, tiled=True)  42.1 us
    unnamed x26, local copies, waits for them, and re-layouts  41.3 us
    psum x1, waiting for transfers between devices, body(): lax.psum(projected.astype(jnp.bfloat16), 'rep').astype(jnp.float32)  37 us
    unnamed x8, waiting for transfers between devices  28.5 us
    all_gather x1, waiting for transfers between devices, body(): lax.all_gather(new_query_w.astype(jnp.bfloat16), 'fs', axis=0, tiled=True)  25.3 us
    all_gather x1, waiting for transfers between devices, body(): lax.all_gather(dir_o, 'fs', axis=0, tiled=True)  23.4 us
    psum x1, blocking collectives, body(): total_squares = lax.psum(local_squares, ('fs', 'tp'))  16.9 us
  transfers between devices with their start and end apart: 7, of which 7 were waited for; matrix products, arithmetic and copies ran while one was open for 12% of the time, Pallas kernels for 0%

commit v1 on v0

--- a/solution.py
+++ b/solution.py
@@ -3,9 +3,15 @@
 import jax.numpy as jnp
 from jax import lax
 from jax.sharding import PartitionSpec as P
+from jax.lax import all_gather
 
 RANK = 512
 HQ = 1024
+
+
+def wait_the_outputs(vector):
+    carry_in = all_gather(vector, "rep")
+    return jnp.sum(carry_in, axis=0)
 
 
 def contract_rows(left_side, right_side):
@@ -65,7 +71,7 @@
     projected = lax.psum_scatter(
         partial_value.astype(jnp.bfloat16), "fs", scatter_dimension=0, tiled=True
     ).astype(jnp.float32)
-    projected = lax.psum(projected.astype(jnp.bfloat16), "rep").astype(jnp.float32) * scale_tokens
+    projected = wait_the_outputs(projected.astype(jnp.bfloat16)).astype(jnp.float32) * scale_tokens
     proj_q = projected[:, :heads_local]
     proj_o = projected[:, heads_local:]
     new_first_q = 0.8 * first_q + 0.2 * proj_q

time: 344 us -> 330 us (0.959)
  waiting for transfers between devices: 244 us -> 226 us
    psum x1 -> x0, waiting for transfers between devices: 37 us -> none  [body(): lax.psum(projected.astype(jnp.bfloat16), 'rep').astype(jnp.float32)]
    all_gather x0 -> x1, waiting for transfers between devices: none -> 19.2 us  [wait_the_outputs(): carry_in = all_gather(vector, 'rep')]
where the time goes in v1:
time: 330 us; the launch traced here: 329 us
  waiting for transfers between devices  226 us (68%)
  local copies, waits for them, and re-layouts  43.5 us (13%)
  blocking collectives  17.3 us (5%)
  matrix products  16.8 us (5%)
  between operations  16.2 us (5%)
  other arithmetic  9.01 us (3%)
    reduce_scatter x1, waiting for transfers between devices, body(): lax.psum_scatter(jnp.concatenate([contract_rows(input_act, query_cot), co...  79.6 us
    all_gather x1, waiting for transfers between devices, body(): lax.all_gather(new_out_w.astype(jnp.bfloat16), 'fs', axis=1, tiled=True)  42.1 us
    unnamed x26, local copies, waits for them, and re-layouts  41.3 us
    unnamed x8, waiting for transfers between devices  28.5 us
    all_gather x1, waiting for transfers between devices, body(): lax.all_gather(new_query_w.astype(jnp.bfloat16), 'fs', axis=0, tiled=True)  25.3 us
    all_gather x1, waiting for transfers between devices, body(): lax.all_gather(dir_o, 'fs', axis=0, tiled=True)  23.2 us
    all_gather x1, waiting for transfers between devices, wait_the_outputs(): carry_in = all_gather(vector, 'rep')  19.2 us
    psum x1, blocking collectives, body(): total_squares = lax.psum(local_squares, ('fs', 'tp'))  17.3 us
  transfers between devices with their start and end apart: 7, of which 7 were waited for; matrix products, arithmetic and copies ran while one was open for 12% of the time, Pallas kernels for 0%

profile of v1, /device:TPU:0, one launch (start us, length us, event | category | flops | bytes accessed | tf_op | source)
XLA Modules:
  0.0 329.3 jit_solution(9477046699237755518)
XLA Ops:
  7.2 1.8 copy-done
  9.1 3.1 convolution_convert_fusion.1
  12.2 1.9 convolution_convert_fusion
  14.1 2.5 pad_maximum_fusion
  16.8 79.6 %reduce-scatter.5.cloned.1.call-done = bf16[512,1024]{0,1:T(8,128)(2,1)} async-done(((bf16[2048,1024]{0,1:T(8,128)(2,1)}), bf16[512,1024]{0,1:T(8,128)(2,1)}) %reduce-scatter.5.cloned.1.call-update) | async-done | bytes 1048592 | tf_op jit(solution)/shard_map/reduce_scatter | solution.py:56
  100.7 2.3 copy.51
  103.0 27.9 %reduce-scatter.7.cloned.1.call-done = bf16[128,1024]{1,0:T(8,128)(2,1)} async-done(((bf16[512,1024]{1,0:T(8,128)(2,1)}), bf16[128,1024]{1,0:T(8,128)(2,1)}) %reduce-scatter.7.cloned.1.call-update) | async-done | bytes 262160
  130.9 1.8 copy.52
  133.7 1.8 copy.33
  137.2 1.8 copy.35
  139.0 19.2 %all-gather.15.cloned.1.call-done = bf16[512,1024]{0,1:T(8,128)(2,1)} async-done(((bf16[128,1024]{0,1:T(8,128)(2,1)}), bf16[512,1024]{0,1:T(8,128)(2,1)}) %all-gather.15.cloned.1.call-update) | async-done | bytes 1048592 | tf_op jit(solution)/shard_map/all_gather | solution.py:13
  158.2 2.1 reshape.20
  160.4 2.5 reduce_sum.30
  162.9 2.9 multiply_reduce_fusion
  167.8 2.5 copy.37
  170.3 17.3 %psum.7 = f32[]{:T(128)} all-reduce(f32[]{:T(128)S(6)} %add.28), channel_id=1, replica_groups=mesh['fs'=4,'rep'=4,'tp'=2] {'fs','tp'}, use_global_device_ids=true, to_apply=%region_5.0 | all-reduce | flops 1 | bytes 8 | tf_op jit(solution)/shard_map/psum | solution.py:84
  188.3 7.9 %all-gather.7.cloned.1.call-done = f32[512,512]{0,1:T(8,128)} async-done(((f32[128,512]{0,1:T(8,128)}), f32[512,512]{0,1:T(8,128)}) %all-gather.7.cloned.1.call-update) | async-done | bytes 1048592 | tf_op jit(solution)/shard_map/all_gather | solution.py:87
  196.2 4.2 %fusion.8 = (bf16[512,512]{0,1:T(8,128)(2,1)}, f32[512,512]{0,1:T(8,128)}, f32[512,512]{0,1:T(8,128)}) fusion(f32[512,512]{0,1:T(8,128)} %copy.37, f32[]{:T(128)S(6)} %sqrt.11, f32[512,512]{0,1:T(8,128)} %all-gather.7.cloned.1.call-done, bf16[512,512]{1,0:T(8,128)(2,1)} %param.18), kind=kOutput, calls=%fused_computation.27 | convolution fusion | flops 1611661312 | bytes 5242884 | tf_op jit(solution)/shard_map/dot_general | solution.py:34
  200.7 2.5 copy.39
  203.2 23.2 %all-gather.9.cloned.1.call-done = f32[512,512]{0,1:T(8,128)} async-done(((f32[128,512]{0,1:T(8,128)}), f32[512,512]{0,1:T(8,128)}) %all-gather.9.cloned.1.call-update) | async-done | bytes 1048592 | tf_op jit(solution)/shard_map/all_gather | solution.py:88
  226.5 4.3 %fusion.7 = (bf16[512,512]{0,1:T(8,128)(2,1)}, f32[512,512]{0,1:T(8,128)}, f32[512,512]{0,1:T(8,128)}) fusion(f32[512,512]{0,1:T(8,128)} %copy.39, f32[]{:T(128)S(6)} %sqrt.11, f32[512,512]{0,1:T(8,128)} %all-gather.9.cloned.1.call-done, bf16[512,512]{1,0:T(8,128)(2,1)} %param.19), kind=kOutput, calls=%fused_computation.26 | convolution fusion | flops 1611661312 | bytes 5242884 | tf_op jit(solution)/shard_map/dot_general | solution.py:34
  230.8 1.8 copy.47
  232.6 1.8 copy.46
  234.4 1.8 copy.45
  237.0 2.5 copy.41
  239.5 2.5 copy.43
  242.0 2.5 copy.40
  244.6 2.5 copy.42
  247.1 25.3 %all-gather.11.cloned.1.call-done = bf16[2048,512]{0,1:T(8,128)(2,1)} async-done(((bf16[512,512]{0,1:T(8,128)(2,1)}), bf16[2048,512]{0,1:T(8,128)(2,1)}) %all-gather.11.cloned.1.call-update) | async-done | bytes 2097168 | tf_op jit(solution)/shard_map/all_gather | solution.py:94
  272.4 3.9 %copy.48 = bf16[2048,512]{1,0:T(8,128)(2,1)} copy(bf16[2048,512]{0,1:T(8,128)(2,1)} %all-gather.11.cloned.1.call-done) | data formatting | bytes 4194304
  276.4 42.1 %all-gather.13.cloned.1.call-done = bf16[512,2048]{0,1:T(8,128)(2,1)} async-done(((bf16[512,512]{0,1:T(8,128)(2,1)}), bf16[512,2048]{0,1:T(8,128)(2,1)}) %all-gather.13.cloned.1.call-update) | async-done | bytes 2097168 | tf_op jit(solution)/shard_map/all_gather | solution.py:95
  318.5 3.9 %copy.49 = bf16[512,2048]{1,0:T(8,128)(2,1)} copy(bf16[512,2048]{0,1:T(8,128)(2,1)} %all-gather.13.cloned.1.call-done) | data formatting | bytes 4194304
  (28 shorter events, 8.9 us)
Async XLA Ops:
  7.2 1.9 copy-start
  7.2 89.2 %reduce-scatter.5.cloned.1.call-start = ((), (), s32[]{:S(2)}) async-start(), calls=%async_computation.2 | async-start | bytes 5242880 | tf_op jit(solution)/shard_map/reduce_scatter | solution.py:56
  9.1 3.1 copy-start.2
  9.1 3.1 copy-start.3
  16.7 114.2 %reduce-scatter.7.cloned.1.call-start = ((), (), s32[]{:S(2)}) async-start(), calls=%async_computation.8 | async-start | bytes 1310720
  99.7 33.2 %copy-start.1 = (f32[128,512]{1,0:T(8,128)S(1)}, f32[128,512]{1,0:T(8,128)}, u32[]{:S(2)}) copy-start(f32[128,512]{1,0:T(8,128)} %param.20) | copy-start | bytes 786436
  103.0 55.2 %all-gather.15.cloned.1.call-start = ((), (), s32[]{:S(2)}) async-start(), calls=%async_computation.7 | async-start | bytes 1310720 | tf_op jit(solution)/shard_map/all_gather | solution.py:13
  132.8 63.5 %all-gather.7.cloned.1.call-start = ((), (), s32[]{:S(2)}) async-start(), calls=%async_computation.3 | async-start | bytes 1310720 | tf_op jit(solution)/shard_map/all_gather | solution.py:87
  165.8 60.6 %all-gather.9.cloned.1.call-start = ((), (), s32[]{:S(2)}) async-start(), calls=%async_computation.4 | async-start | bytes 1310720 | tf_op jit(solution)/shard_map/all_gather | solution.py:88
  166.4 106.0 %all-gather.11.cloned.1.call-start = ((), (), s32[]{:S(2)}) async-start(), calls=%async_computation.5 | async-start | bytes 2621440 | tf_op jit(solution)/shard_map/all_gather | solution.py:94
  200.5 118.0 %all-gather.13.cloned.1.call-start = ((), (), s32[]{:S(2)}) async-start(), calls=%async_computation.6 | async-start | bytes 2621440 | tf_op jit(solution)/shard_map/all_gather | solution.py:95
Sparse Core Ops, SparseCore 0:
  16.8 79.5 reduce-scatter.4
  103.1 27.7 reduce-scatter.6
  133.3 24.8 all-gather.14
  166.0 30.2 all-gather.6
  198.2 28.2 all-gather.8
  228.5 43.9 all-gather.10
  274.0 44.4 all-gather.12
